TPU v7x, 32 devices: a whole 2x2x4 slice. The times are simulated.
32 devices in a mesh: grp: 2 (over y), fs: 4 (over z), tp: 4 (over x, core).
Axes of the slice: x: 2, y: 2, z: 4, core: 2. Of those that a mesh axis runs over, the one named last changes fastest.
Arguments:
- prompt_rows: bfloat16 [8192, 2048], P(('grp', 'fs')), parts along dimension 0, may hold values from -6 to 6
- up_master: float32 [2048, 8192], P('fs', 'tp'), may hold values from -0.125 to 0.125
- down_master: float32 [8192, 2048], P('fs', 'tp'), may hold values from -0.0625 to 0.0625
- norm_gain: float32 [2048], P('fs'), may hold values from 0.1 to 1.9
Outputs:
- up_sampler: bfloat16 [8, 2048, 2048], P(('grp', 'tp')), parts along dimension 0
- down_sampler: bfloat16 [8, 2048, 2048], P(('grp', 'tp')), parts along dimension 0
- layer_out: bfloat16 [8192, 2048], P(('grp', 'fs', 'tp')), parts along dimension 0
There are 2 independent parts, one for each index of `grp`. A program takes and returns all parts, laid end to end along the dimension named above; an argument that names none is the same for every part. Nothing has to cross between parts.
All inputs are finite; a program needn't handle non-finite values.
Results may differ from a plain program's by a relative error of at most 0.014.
Values may be sent and summed in bfloat16 or wider, within the bound.
A program may use at most 128 MiB of HBM per device.

v0:
```python
import jax
import jax.numpy as jnp
from jax import lax
from jax.sharding import PartitionSpec as P

eps = 1e-06


def on_device(prompt_rows, up_master, down_master, norm_gain):
    fs_count = lax.axis_size("fs")
    tp_count = lax.axis_size("tp")
    fs_per_tp = fs_count // tp_count
    up_cast = (up_master * norm_gain[:, None]).astype(jnp.bfloat16)
    down_cast = down_master.astype(jnp.bfloat16)
    up_local_rows = up_cast.shape[0]
    local_width = up_cast.shape[1]
    unit_span = local_width // fs_count
    down_local_cols = down_cast.shape[1]
    full_width = down_local_cols * tp_count
    values = prompt_rows.astype(jnp.float32)
    normed = (values * lax.rsqrt(jnp.mean(values * values, axis=-1, keepdims=True) + eps)).astype(
        jnp.bfloat16
    )
    up_parts = up_cast.reshape(up_local_rows, fs_per_tp, tp_count, unit_span)
    up_local = lax.all_to_all(up_parts, "tp", split_axis=2, concat_axis=1, tiled=True).reshape(
        up_local_rows, local_width
    )
    up_sampler = lax.all_gather(up_local, "fs", axis=0, tiled=True)
    down_parts = down_cast.reshape(tp_count, unit_span, down_local_cols)
    down_local = lax.all_to_all(down_parts, "tp", split_axis=0, concat_axis=2, tiled=True).reshape(
        unit_span, full_width
    )
    down_sampler = lax.all_gather(down_local, "fs", axis=0, tiled=True)
    pre_act = jnp.dot(normed, up_sampler, preferred_element_type=jnp.float32)
    hidden = jnp.square(jax.nn.relu(pre_act)).astype(jnp.bfloat16)
    summed = lax.psum_scatter(
        jnp.dot(hidden, down_sampler, preferred_element_type=jnp.float32).astype(jnp.bfloat16),
        "tp",
        scatter_dimension=0,
        tiled=True,
    )
    return (up_sampler[None], down_sampler[None], summed)


def solution(mesh):
    in_specs = (P(("grp", "fs"), None), P("fs", "tp"), P("fs", "tp"), P("fs"))
    out_specs = (
        P(("grp", "tp"), None, None),
        P(("grp", "tp"), None, None),
        P(("grp", "fs", "tp"), None),
    )
    return jax.shard_map(
        on_device, mesh=mesh, in_specs=in_specs, out_specs=out_specs, check_vma=False
    )
```

profile of v0, /device:TPU:0, one launch (start us, length us, event | category | flops | bytes accessed | tf_op | source)
XLA Modules:
  0.0 416.7 jit_solution(6983446177385879946)
XLA Ops:
  7.2 0.0 all-gather.5.cloned.1.call-start
  7.2 2.5 convert_element_type.19
  9.7 29.7 %all_to_all.24 = bf16[4,512,512]{2,1,0:T(8,128)(2,1)S(1)} all-to-all(bf16[4,512,512]{2,1,0:T(8,128)(2,1)S(1)} %bitcast.12), channel_id=1, replica_groups=mesh['grp'=2,'fs'=4,'tp'=4] {'tp'}, dimensions={0} | all-to-all | bytes 4194304 | tf_op jit(solution)/shard_map/all_to_all | solution.py:30
  39.4 2.4 copy.11
  41.7 0.0 all-gather.5.cloned.1.call-update
  41.8 0.0 copy-start
  41.8 0.0 all-gather.3.cloned.1.call-start
  41.8 5.3 %copy.8 = f32[512,2048]{0,1:T(8,128)} copy(f32[512,2048]{1,0:T(8,128)} %param.5) | data formatting | bytes 8388608 | tf_op args[1]
  47.2 0.0 copy-done
  47.2 3.1 multiply_convert_fusion.1
  50.3 2.4 copy.9
  52.6 29.3 %all_to_all.25 = bf16[512,1,4,512]{3,0,1,2:T(8,128)(2,1)S(1)} all-to-all(bf16[512,1,4,512]{3,0,1,2:T(8,128)(2,1)} %copy.9), channel_id=1, replica_groups=mesh['grp'=2,'fs'=4,'tp'=4] {'tp'}, dimensions={2} | all-to-all | bytes 4194304 | tf_op jit(solution)/shard_map/all_to_all | solution.py:25
  81.9 2.4 copy.10
  84.3 0.0 all-gather.3.cloned.1.call-update
  84.3 0.0 reduce-scatter.2.cloned.1.call-start
  84.4 3.1 fusion
  87.5 104.3 %all-gather.5.cloned.1.call-done = bf16[2048,2048]{0,1:T(8,128)(2,1)} async-done(((bf16[512,2048]{0,1:T(8,128)(2,1)}), bf16[2048,2048]{0,1:T(8,128)(2,1)}) %all-gather.5.cloned.1.call-update) | async-done | bytes 8388624 | tf_op jit(solution)/shard_map/all_gather | solution.py:33
  191.8 150.0 %all-gather.3.cloned.1.call-done = bf16[2048,2048]{0,1:T(8,128)(2,1)} async-done(((bf16[512,2048]{0,1:T(8,128)(2,1)}), bf16[2048,2048]{0,1:T(8,128)(2,1)}) %all-gather.3.cloned.1.call-update) | async-done | bytes 8388624 | tf_op jit(solution)/shard_map/all_gather | solution.py:28
  341.8 25.4 %fusion.9 = bf16[1024,2048]{1,0:T(8,128)(2,1)} fusion(bf16[2048,2048]{0,1:T(8,128)(2,1)} %all-gather.5.cloned.1.call-done, bf16[2048,2048]{0,1:T(8,128)(2,1)} %all-gather.3.cloned.1.call-done, bf16[1024,2048]{1,0:T(8,128)(2,1)} %param.4, f32[1024]{0:T(1024)S(1)} %add_rsqrt_fusion), kind=kOutput, calls=%fused_computation.9 | convolution fusion | flops 17194549248 | bytes 25169920 | tf_op jit(solution)/shard_map/dot_general | solution.py:37
  367.2 0.0 reduce-scatter.2.cloned.1.call-update
  367.3 12.3 %copy.12 = bf16[1,2048,2048]{2,1,0:T(8,128)(2,1)} copy(bf16[1,2048,2048]{1,2,0:T(8,128)(2,1)} %bitcast.14) | data formatting | bytes 16777216
  379.6 12.0 %copy.13 = bf16[1,2048,2048]{2,1,0:T(8,128)(2,1)} copy(bf16[1,2048,2048]{1,2,0:T(8,128)(2,1)} %bitcast.13) | data formatting | bytes 16777216
  391.5 18.6 %reduce-scatter.2.cloned.1.call-done = bf16[256,2048]{1,0:T(8,128)(2,1)} async-done(((bf16[1024,2048]{1,0:T(8,128)(2,1)}), bf16[256,2048]{1,0:T(8,128)(2,1)}) %reduce-scatter.2.cloned.1.call-update) | async-done | bytes 1048592 | tf_op jit(solution)/shard_map/reduce_scatter | solution.py:36
  (1 shorter events, 0.0 us)
Async XLA Ops:
  7.2 184.7 %all-gather.5.cloned.1.call-start = ((), (), s32[]{:S(2)}) async-start(), calls=%async_computation.4 | async-start | bytes 10485760 | tf_op jit(solution)/shard_map/all_gather | solution.py:33
  41.8 5.4 %copy-start = (f32[512]{0:T(512)S(1)}, f32[512]{0:T(512)}, u32[]{:S(2)}) copy-start(f32[512]{0:T(512)} %param.7) | copy-start | bytes 6148
  41.8 300.0 %all-gather.3.cloned.1.call-start = ((), (), s32[]{:S(2)}) async-start(), calls=%async_computation.3 | async-start | bytes 10485760 | tf_op jit(solution)/shard_map/all_gather | solution.py:28
  84.3 325.9 %reduce-scatter.2.cloned.1.call-start = ((), (), s32[]{:S(2)}) async-start(), calls=%async_computation.5 | async-start | bytes 5242880 | tf_op jit(solution)/shard_map/reduce_scatter | solution.py:36
Sparse Core Ops, SparseCore 0:
  41.9 149.9 all-gather.4
  194.0 147.7 all-gather.2
  367.4 42.7 reduce-scatter.1
where the time goes:
time: 418 us; the launch traced here: 417 us
  waiting for transfers between devices  273 us (65%)
  blocking collectives  59 us (14%)
  local copies, waits for them, and re-layouts  36.7 us (9%)
  matrix products  25.4 us (6%)
  between operations  13.8 us (3%)
  other arithmetic  8.69 us (2%)
    all_gather x1, waiting for transfers between devices, on_device(): up_sampler = lax.all_gather(up_local, 'fs', axis=0, tiled=True)  150 us
    all_gather x1, waiting for transfers between devices, on_device(): down_sampler = lax.all_gather(down_local, 'fs', axis=0, tiled=True)  104 us
    all_to_all x1, blocking collectives, on_device(): lax.all_to_all(down_parts, 'tp', split_axis=0, concat_axis=2, tiled=True)  29.7 us
    unnamed x5, local copies, waits for them, and re-layouts  29.7 us
    all_to_all x1, blocking collectives, on_device(): lax.all_to_all(up_parts, 'tp', split_axis=2, concat_axis=1, tiled=True)  29.3 us
    dot_general x1, matrix products, on_device(): jnp.dot(hidden, down_sampler, preferred_element_type=jnp.float32)  25.4 us
    reduce_scatter x1, waiting for transfers between devices, on_device(): lax.psum_scatter(jnp.dot(hidden, down_sampler, preferred_element_type=jnp...  18.6 us
  transfers between devices with their start and end apart: 3, of which 3 were waited for; matrix products, arithmetic and copies ran while one was open for 10% of the time, Pallas kernels for 0%

commit v1 on v0

--- a/solution.py
+++ b/solution.py
@@ -30,7 +30,8 @@
     down_local = lax.all_to_all(down_parts, "tp", split_axis=0, concat_axis=2, tiled=True).reshape(
         unit_span, full_width
     )
-    down_sampler = lax.all_gather(down_local, "fs", axis=0, tiled=True)
+    stack = jnp.stack([down_local] * lax.axis_size("fs"))
+    down_sampler = jnp.concatenate(lax.all_to_all(stack, "fs", 0, 0), axis=0)
     pre_act = jnp.dot(normed, up_sampler, preferred_element_type=jnp.float32)
     hidden = jnp.square(jax.nn.relu(pre_act)).astype(jnp.bfloat16)
     summed = lax.psum_scatter(

time: 418 us -> 489 us (1.17)
  waiting for transfers between devices: 273 us -> 378 us
  blocking collectives: 59 us -> 0 us
  starting transfers between devices: 0.12 us -> 14.7 us
  local copies, waits for them, and re-layouts: 36.7 us -> 44.2 us
    all_gather x1, waiting for transfers between devices: 150 us -> 294 us  [on_device(): up_sampler = lax.all_gather(up_local, 'fs', axis=0, tiled=True)]
    all_gather x1 -> x0, waiting for transfers between devices: 104 us -> none  [on_device(): down_sampler = lax.all_gather(down_local, 'fs', axis=0, tiled=True)]
    all_to_all x2 -> x0, blocking collectives: 59 us -> none  [the longest x1 29.7 us: on_device(): lax.all_to_all(down_parts, 'tp', split_axis=0, concat_axis=2, tiled=True)]
    all_to_all x0 -> x3, waiting for transfers between devices: none -> 53.6 us  [the longest x1 21.1 us: on_device(): down_sampler = jnp.concatenate(lax.all_to_all(stack, 'fs', 0, 0), axis=0)]
    all_to_all x0 -> x3, starting transfers between devices: none -> 14.5 us  [the longest x1 5.79 us: on_device(): down_sampler = jnp.concatenate(lax.all_to_all(stack, 'fs', 0, 0), axis=0)]
    reduce_scatter x1, waiting for transfers between devices: 18.6 us -> 30.7 us  [on_device(): lax.psum_scatter(jnp.dot(hidden, down_sampler, preferred_element_type=jnp...]
  transfers between devices with their start and end apart: 3 -> 5, of which waited for: 3 -> 5; matrix products, arithmetic and copies ran while one was open for 10% -> 8% of each run, Pallas kernels for 0% -> 0%
where the time goes in v1:
time: 489 us; the launch traced here: 488 us
  waiting for transfers between devices  378 us (77%)
  local copies, waits for them, and re-layouts  44.2 us (9%)
  matrix products  25.6 us (5%)
  starting transfers between devices  14.7 us (3%)
  between operations  14.1 us (3%)
  other arithmetic  11.3 us (2%)
    all_gather x1, waiting for transfers between devices, on_device(): up_sampler = lax.all_gather(up_local, 'fs', axis=0, tiled=True)  294 us
    reduce_scatter x1, waiting for transfers between devices, on_device(): lax.psum_scatter(jnp.dot(hidden, down_sampler, preferred_element_type=jnp...  30.7 us
    unnamed x5, local copies, waits for them, and re-layouts  26.1 us
    dot_general x1, matrix products, on_device(): jnp.dot(hidden, down_sampler, preferred_element_type=jnp.float32)  25.6 us
    all_to_all x1, waiting for transfers between devices, on_device(): down_sampler = jnp.concatenate(lax.all_to_all(stack, 'fs', 0, 0), axis=0)  21.1 us
    all_to_all x1, waiting for transfers between devices, on_device(): lax.all_to_all(up_parts, 'tp', split_axis=2, concat_axis=1, tiled=True)  20.4 us
    all_to_all x1, waiting for transfers between devices, on_device(): lax.all_to_all(down_parts, 'tp', split_axis=0, concat_axis=2, tiled=True)  12.1 us
  transfers between devices with their start and end apart: 5, of which 5 were waited for; matrix products, arithmetic and copies ran while one was open for 8% of the time, Pallas kernels for 0%

profile of v1, /device:TPU:0, one launch (start us, length us, event | category | flops | bytes accessed | tf_op | source)
XLA Modules:
  0.0 488.0 jit_solution(8762681000412079163)
XLA Ops:
  7.2 3.8 convert_element_type.19
  11.0 4.2 all-to-all-start.1
  15.2 0.0 copy-start
  15.2 5.3 %copy.12 = f32[512,2048]{0,1:T(8,128)} copy(f32[512,2048]{1,0:T(8,128)} %param.5) | data formatting | bytes 8388608 | tf_op args[1]
  20.6 0.0 copy-done
  20.6 4.1 multiply_convert_fusion.1
  24.6 4.1 copy.13
  28.8 12.1 %all-to-all-done.1 = bf16[4,512,512]{2,1,0:T(8,128)(2,1)S(1)} async-done(((bf16[4,512,512]{2,1,0:T(8,128)(2,1)}), bf16[4,512,512]{2,1,0:T(8,128)(2,1)S(1)}, u32[]{:S(2)}, u32[]{:S(2)}) %all-to-all-start.1) | async-done | bytes 2097184 | tf_op jit(solution)/shard_map/all_to_all | solution.py:30
  40.9 4.4 all-to-all-start
  45.3 0.0 all-gather.2.cloned.1.call-start
  45.4 2.4 copy.15
  47.7 2.9 copy.16
  50.7 20.4 %all-to-all-done = bf16[512,1,4,512]{3,0,1,2:T(8,128)(2,1)} async-done(((bf16[512,1,4,512]{3,0,1,2:T(8,128)(2,1)}), bf16[512,1,4,512]{3,0,1,2:T(8,128)(2,1)}, u32[]{:S(2)}, u32[]{:S(2)}) %all-to-all-start) | async-done | bytes 2097184 | tf_op jit(solution)/shard_map/all_to_all | solution.py:25
  71.1 4.1 copy.14
  75.2 0.0 all-gather.2.cloned.1.call-update
  75.2 4.5 stack.3
  79.7 5.8 %all-to-all-start.2 = ((bf16[4,512,2048]{2,1,0:T(8,128)(2,1)}), bf16[4,512,2048]{2,1,0:T(8,128)(2,1)}, u32[]{:S(2)}, u32[]{:S(2)}) async-start(bf16[4,512,2048]{2,1,0:T(8,128)(2,1)} %stack.3), calls=%async_computation.2 | async-start | bytes 16777216 | tf_op jit(solution)/shard_map/all_to_all | solution.py:34
  85.5 0.2 reduce-scatter.2.cloned.1.call-start
  85.7 3.4 fusion
  89.1 293.9 %all-gather.2.cloned.1.call-done = bf16[2048,2048]{0,1:T(8,128)(2,1)} async-done(((bf16[512,2048]{0,1:T(8,128)(2,1)}), bf16[2048,2048]{0,1:T(8,128)(2,1)}) %all-gather.2.cloned.1.call-update) | async-done | bytes 8388624 | tf_op jit(solution)/shard_map/all_gather | solution.py:28
  383.0 21.1 %all-to-all-done.2 = bf16[4,512,2048]{2,1,0:T(8,128)(2,1)} async-done(((bf16[4,512,2048]{2,1,0:T(8,128)(2,1)}), bf16[4,512,2048]{2,1,0:T(8,128)(2,1)}, u32[]{:S(2)}, u32[]{:S(2)}) %all-to-all-start.2) | async-done | bytes 8388640 | tf_op jit(solution)/shard_map/all_to_all | solution.py:34
  404.1 25.6 %fusion.9 = bf16[1024,2048]{1,0:T(8,128)(2,1)} fusion(bf16[2048,2048]{1,0:T(8,128)(2,1)} %bitcast.8, bf16[2048,2048]{0,1:T(8,128)(2,1)} %all-gather.2.cloned.1.call-done, bf16[1024,2048]{1,0:T(8,128)(2,1)} %param.4, f32[1024]{0:T(1024)S(1)} %add_rsqrt_fusion), kind=kOutput, calls=%fused_computation.9 | convolution fusion | flops 17194549248 | bytes 25169920 | tf_op jit(solution)/shard_map/dot_general | solution.py:38
  429.7 0.0 reduce-scatter.2.cloned.1.call-update
  429.7 12.4 %copy.17 = bf16[1,2048,2048]{2,1,0:T(8,128)(2,1)} copy(bf16[1,2048,2048]{1,2,0:T(8,128)(2,1)} %bitcast.12) | data formatting | bytes 16777216
  442.1 30.7 %reduce-scatter.2.cloned.1.call-done = bf16[256,2048]{1,0:T(8,128)(2,1)} async-done(((bf16[1024,2048]{1,0:T(8,128)(2,1)}), bf16[256,2048]{1,0:T(8,128)(2,1)}) %reduce-scatter.2.cloned.1.call-update) | async-done | bytes 1048592 | tf_op jit(solution)/shard_map/reduce_scatter | solution.py:37
  472.8 8.4 %copy.19 = bf16[1,2048,2048]{2,1,0:T(8,128)(2,1)} copy(bf16[1,2048,2048]{2,1,0:T(8,128)(2,1)} %bitcast.7) | data formatting | bytes 16777216
  (1 shorter events, 0.0 us)
Async XLA Ops:
  11.0 29.9 %all-to-all-start.1 = ((bf16[4,512,512]{2,1,0:T(8,128)(2,1)}), bf16[4,512,512]{2,1,0:T(8,128)(2,1)S(1)}, u32[]{:S(2)}, u32[]{:S(2)}) async-start(bf16[4,512,512]{2,1,0:T(8,128)(2,1)} %bitcast.3), calls=%async_computation.1 | async-start | bytes 4194304 | tf_op jit(solution)/shard_map/all_to_all | solution.py:30
  15.2 5.4 %copy-start = (f32[512]{0:T(512)S(1)}, f32[512]{0:T(512)}, u32[]{:S(2)}) copy-start(f32[512]{0:T(512)} %param.7) | copy-start | bytes 6148
  40.9 30.2 %all-to-all-start = ((bf16[512,1,4,512]{3,0,1,2:T(8,128)(2,1)}), bf16[512,1,4,512]{3,0,1,2:T(8,128)(2,1)}, u32[]{:S(2)}, u32[]{:S(2)}) async-start(bf16[512,1,4,512]{3,0,1,2:T(8,128)(2,1)} %copy.13), calls=%async_computation | async-start | bytes 4194304 | tf_op jit(solution)/shard_map/all_to_all | solution.py:25
  45.3 337.7 %all-gather.2.cloned.1.call-start = ((), (), s32[]{:S(2)}) async-start(), calls=%async_computation.4 | async-start | bytes 10485760 | tf_op jit(solution)/shard_map/all_gather | solution.py:28
  79.7 324.4 %all-to-all-start.2 = ((bf16[4,512,2048]{2,1,0:T(8,128)(2,1)}), bf16[4,512,2048]{2,1,0:T(8,128)(2,1)}, u32[]{:S(2)}, u32[]{:S(2)}) async-start(bf16[4,512,2048]{2,1,0:T(8,128)(2,1)} %stack.3), calls=%async_computation.2 | async-start | bytes 16777216 | tf_op jit(solution)/shard_map/all_to_all | solution.py:34
  85.5 387.3 %reduce-scatter.2.cloned.1.call-start = ((), (), s32[]{:S(2)}) async-start(), calls=%async_computation.5 | async-start | bytes 5242880 | tf_op jit(solution)/shard_map/reduce_scatter | solution.py:37
Sparse Core Ops, SparseCore 0:
  75.3 307.6 all-gather.1
  429.9 42.8 reduce-scatter.1

commit v2 on v0

--- a/solution.py
+++ b/solution.py
@@ -4,6 +4,16 @@
 from jax.sharding import PartitionSpec as P
 
 eps = 1e-06
+
+
+def search_the_series(slab_in, block_here, named_axis):
+    return jnp.split(
+        jax.lax.all_gather(
+            jnp.concatenate([slab_in, block_here], axis=1), axis_name=named_axis, axis=0, tiled=True
+        ),
+        [slab_in.shape[1]],
+        1,
+    )
 
 
 def on_device(prompt_rows, up_master, down_master, norm_gain):
@@ -25,12 +35,11 @@
     up_local = lax.all_to_all(up_parts, "tp", split_axis=2, concat_axis=1, tiled=True).reshape(
         up_local_rows, local_width
     )
-    up_sampler = lax.all_gather(up_local, "fs", axis=0, tiled=True)
     down_parts = down_cast.reshape(tp_count, unit_span, down_local_cols)
     down_local = lax.all_to_all(down_parts, "tp", split_axis=0, concat_axis=2, tiled=True).reshape(
         unit_span, full_width
     )
-    down_sampler = lax.all_gather(down_local, "fs", axis=0, tiled=True)
+    up_sampler, down_sampler = search_the_series(up_local, down_local, "fs")
     pre_act = jnp.dot(normed, up_sampler, preferred_element_type=jnp.float32)
     hidden = jnp.square(jax.nn.relu(pre_act)).astype(jnp.bfloat16)
     summed = lax.psum_scatter(

time: 418 us -> 443 us (1.060)
  blocking collectives: 59 us -> 0 us
  waiting for transfers between devices: 273 us -> 326 us
  local copies, waits for them, and re-layouts: 36.7 us -> 53 us
  starting transfers between devices: 0.12 us -> 8.77 us
  other arithmetic: 8.69 us -> 14.8 us
    all_to_all x2 -> x0, blocking collectives: 59 us -> none  [the longest x1 29.7 us: on_device(): lax.all_to_all(down_parts, 'tp', split_axis=0, concat_axis=2, tiled=True)]
    all_to_all x0 -> x2, waiting for transfers between devices: none -> 35.4 us  [the longest x1 23.3 us: on_device(): lax.all_to_all(up_parts, 'tp', split_axis=2, concat_axis=1, tiled=True)]
    all_gather x2 -> x1, waiting for transfers between devices: 254 us -> 285 us  [search_the_series(): jax.lax.all_gather(jnp.concatenate([slab_in, block_here], axis=1), axis_n...]
    reduce_scatter x1, waiting for transfers between devices: 18.6 us -> 5.96 us  [on_device(): lax.psum_scatter(jnp.dot(hidden, down_sampler, preferred_element_type=jnp...]
    broadcast_in_dim x0 -> x1, local copies, waits for them, and re-layouts: none -> 12.5 us  [on_device(): return (up_sampler[None], down_sampler[None], summed)]
    all_to_all x0 -> x2, starting transfers between devices: none -> 8.69 us  [the longest x1 4.45 us: on_device(): lax.all_to_all(up_parts, 'tp', split_axis=2, concat_axis=1, tiled=True)]
    unnamed x5 -> x7, local copies, waits for them, and re-layouts: 29.7 us -> 29.8 us
  transfers between devices with their start and end apart: 3 -> 4, of which waited for: 3 -> 4; matrix products, arithmetic and copies ran while one was open for 10% -> 13% of each run, Pallas kernels for 0% -> 0%
where the time goes in v2:
time: 443 us; the launch traced here: 442 us
  waiting for transfers between devices  326 us (74%)
  local copies, waits for them, and re-layouts  53 us (12%)
  matrix products  25.1 us (6%)
  other arithmetic  14.8 us (3%)
  between operations  14.1 us (3%)
  starting transfers between devices  8.77 us (2%)
    all_gather x1, waiting for transfers between devices, search_the_series(): jax.lax.all_gather(jnp.concatenate([slab_in, block_here], axis=1), axis_n...  285 us
    unnamed x7, local copies, waits for them, and re-layouts  29.8 us
    dot_general x1, matrix products, on_device(): jnp.dot(hidden, down_sampler, preferred_element_type=jnp.float32)  25.1 us
    all_to_all x1, waiting for transfers between devices, on_device(): lax.all_to_all(up_parts, 'tp', split_axis=2, concat_axis=1, tiled=True)  23.3 us
    broadcast_in_dim x1, local copies, waits for them, and re-layouts, on_device(): return (up_sampler[None], down_sampler[None], summed)  12.5 us
    all_to_all x1, waiting for transfers between devices, on_device(): lax.all_to_all(down_parts, 'tp', split_axis=0, concat_axis=2, tiled=True)  12.1 us
  transfers between devices with their start and end apart: 4, of which 4 were waited for; matrix products, arithmetic and copies ran while one was open for 13% of the time, Pallas kernels for 0%

profile of v2, /device:TPU:0, one launch (start us, length us, event | category | flops | bytes accessed | tf_op | source)
XLA Modules:
  0.0 442.0 jit_solution(1620309905507870245)
XLA Ops:
  7.2 3.8 convert_element_type.19
  10.9 4.2 all-to-all-start.1
  15.2 0.0 copy-start.1
  15.2 5.3 %copy.8 = f32[512,2048]{0,1:T(8,128)} copy(f32[512,2048]{1,0:T(8,128)} %param.5) | data formatting | bytes 8388608 | tf_op args[1]
  20.5 0.0 copy-done.1
  20.5 4.1 multiply_convert_fusion.1
  24.6 4.1 copy.9
  28.7 12.1 %all-to-all-done.1 = bf16[4,512,512]{2,1,0:T(8,128)(2,1)S(1)} async-done(((bf16[4,512,512]{2,1,0:T(8,128)(2,1)}), bf16[4,512,512]{2,1,0:T(8,128)(2,1)S(1)}, u32[]{:S(2)}, u32[]{:S(2)}) %all-to-all-start.1) | async-done | bytes 2097184 | tf_op jit(solution)/shard_map/all_to_all | solution.py:39
  40.9 4.5 %all-to-all-start = ((bf16[512,1,4,512]{3,0,1,2:T(8,128)(2,1)}), bf16[512,1,4,512]{3,0,1,2:T(8,128)(2,1)}, u32[]{:S(2)}, u32[]{:S(2)}) async-start(bf16[512,1,4,512]{3,0,1,2:T(8,128)(2,1)} %copy.9), calls=%async_computation | async-start | bytes 4194304 | tf_op jit(solution)/shard_map/all_to_all | solution.py:35
  45.3 0.0 all-gather.2.cloned.1.call-start
  45.4 2.4 copy.11
  47.7 0.0 copy-start
  47.7 23.3 %all-to-all-done = bf16[512,1,4,512]{3,0,1,2:T(8,128)(2,1)} async-done(((bf16[512,1,4,512]{3,0,1,2:T(8,128)(2,1)}), bf16[512,1,4,512]{3,0,1,2:T(8,128)(2,1)}, u32[]{:S(2)}, u32[]{:S(2)}) %all-to-all-start) | async-done | bytes 2097184 | tf_op jit(solution)/shard_map/all_to_all | solution.py:35
  71.0 4.1 copy.10
  75.2 0.0 copy-done
  75.2 3.9 pad_maximum_fusion
  79.0 0.0 all-gather.2.cloned.1.call-update
  79.1 0.0 reduce-scatter.2.cloned.1.call-start
  79.1 3.1 fusion
  82.2 284.9 %all-gather.2.cloned.1.call-done = bf16[2048,4096]{0,1:T(8,128)(2,1)} async-done(((bf16[512,4096]{0,1:T(8,128)(2,1)}), bf16[2048,4096]{0,1:T(8,128)(2,1)}) %all-gather.2.cloned.1.call-update) | async-done | bytes 16777232 | tf_op jit(solution)/shard_map/all_gather | solution.py:11
  367.1 25.1 %fusion.10 = bf16[1024,2048]{1,0:T(8,128)(2,1)} fusion(bf16[2048,4096]{0,1:T(8,128)(2,1)} %all-gather.2.cloned.1.call-done, bf16[1024,2048]{1,0:T(8,128)(2,1)} %param.4, f32[1024]{0:T(1024)S(1)} %add_rsqrt_fusion), kind=kOutput, calls=%fused_computation.14 | convolution fusion | flops 17194549248 | bytes 25169920 | tf_op jit(solution)/shard_map/dot_general | solution.py:46
  392.2 0.0 reduce-scatter.2.cloned.1.call-update
  392.2 12.5 %slice_bitcast_fusion = (bf16[1,2048,2048]{1,2,0:T(8,128)(2,1)}, bf16[1,2048,2048]{1,2,0:T(8,128)(2,1)}) fusion(bf16[2048,4096]{0,1:T(8,128)(2,1)} %all-gather.2.cloned.1.call-done), kind=kLoop, calls=%fused_computation.7 | loop fusion | bytes 33554432 | tf_op jit(solution)/shard_map/broadcast_in_dim | solution.py:51
  404.7 12.2 %copy.13 = bf16[1,2048,2048]{2,1,0:T(8,128)(2,1)} copy(bf16[1,2048,2048]{1,2,0:T(8,128)(2,1)} %get-tuple-element.6) | data formatting | bytes 16777216
  416.9 12.2 %copy.12 = bf16[1,2048,2048]{2,1,0:T(8,128)(2,1)} copy(bf16[1,2048,2048]{1,2,0:T(8,128)(2,1)} %get-tuple-element.7) | data formatting | bytes 16777216
  429.2 6.0 %reduce-scatter.2.cloned.1.call-done = bf16[256,2048]{1,0:T(8,128)(2,1)} async-done(((bf16[1024,2048]{1,0:T(8,128)(2,1)}), bf16[256,2048]{1,0:T(8,128)(2,1)}) %reduce-scatter.2.cloned.1.call-update) | async-done | bytes 1048592 | tf_op jit(solution)/shard_map/reduce_scatter | solution.py:45
  (1 shorter events, 0.0 us)
Async XLA Ops:
  10.9 29.9 %all-to-all-start.1 = ((bf16[4,512,512]{2,1,0:T(8,128)(2,1)}), bf16[4,512,512]{2,1,0:T(8,128)(2,1)S(1)}, u32[]{:S(2)}, u32[]{:S(2)}) async-start(bf16[4,512,512]{2,1,0:T(8,128)(2,1)} %bitcast.2), calls=%async_computation.1 | async-start | bytes 4194304 | tf_op jit(solution)/shard_map/all_to_all | solution.py:39
  15.2 5.4 %copy-start.1 = (f32[512]{0:T(512)S(1)}, f32[512]{0:T(512)}, u32[]{:S(2)}) copy-start(f32[512]{0:T(512)} %param.7) | copy-start | bytes 6148
  40.9 30.2 %all-to-all-start = ((bf16[512,1,4,512]{3,0,1,2:T(8,128)(2,1)}), bf16[512,1,4,512]{3,0,1,2:T(8,128)(2,1)}, u32[]{:S(2)}, u32[]{:S(2)}) async-start(bf16[512,1,4,512]{3,0,1,2:T(8,128)(2,1)} %copy.9), calls=%async_computation | async-start | bytes 4194304 | tf_op jit(solution)/shard_map/all_to_all | solution.py:35
  45.3 321.8 %all-gather.2.cloned.1.call-start = ((), (), s32[]{:S(2)}) async-start(), calls=%async_computation.3 | async-start | bytes 20971520 | tf_op jit(solution)/shard_map/all_gather | solution.py:11
  47.7 27.4 %copy-start = (bf16[4,512,512]{1,2,0:T(8,128)(2,1)S(1)}, bf16[4,512,512]{1,2,0:T(8,128)(2,1)}, u32[]{:S(2)}) copy-start(bf16[4,512,512]{1,2,0:T(8,128)(2,1)} %copy.11) | copy-start | bytes 6291460
  79.1 356.1 %reduce-scatter.2.cloned.1.call-start = ((), (), s32[]{:S(2)}) async-start(), calls=%async_computation.4 | async-start | bytes 5242880 | tf_op jit(solution)/shard_map/reduce_scatter | solution.py:45
Sparse Core Ops, SparseCore 0:
  79.2 287.8 all-gather.1
  392.3 42.7 reduce-scatter.1
